TPU v7x, 32 devices: a whole 2x2x4 slice. The times are simulated.
32 devices in a mesh: ep: 8 (over z, x), tp: 4 (over y, core).
Axes of the slice: x: 2, y: 2, z: 4, core: 2. Of those that a mesh axis runs over, the one named last changes fastest.
Arguments:
- tokens: bfloat16 [384, 1024], P('ep'), may hold values from -6 to 6
- head_state: float32 [384, 8, 64, 64], P('ep', 'tp'), may hold values from -6 to 6
- recept_weight: bfloat16 [1024, 512], P(None, 'tp'), may hold values from -0.1875 to 0.1875
- key_weight: bfloat16 [1024, 512], P(None, 'tp'), may hold values from -0.1875 to 0.1875
- value_weight: bfloat16 [1024, 512], P(None, 'tp'), may hold values from -0.1875 to 0.1875
- decay_down_factor: bfloat16 [1024, 64], replicated, may hold values from -0.1875 to 0.1875
- decay_up_factor: bfloat16 [64, 512], P(None, 'tp'), may hold values from -0.75 to 0.75
- decay_base: float32 [512], P('tp'), may hold values from -5 to 3
- rate_down_factor: bfloat16 [1024, 64], replicated, may hold values from -0.1875 to 0.1875
- rate_up_factor: bfloat16 [64, 512], P(None, 'tp'), may hold values from -0.75 to 0.75
- rate_base: float32 [512], P('tp'), may hold values from -3 to 3
- head_gain: float32 [512], P('tp'), may hold values from 0.1 to 1.9
- out_weight: bfloat16 [512, 1024], P('tp'), may hold values from -0.25 to 0.25
- route_experts: int32 [384, 4], P('ep'), may hold values from 0 to 7, all different within a row; in each aligned block of 48 rows (0 to 47, 48 to 95, ...) at most 48 rows name the same one
- route_weights: float32 [384, 4], P('ep'), may hold values from 0.03 to 0.2
- expert_gate: bfloat16 [8, 1024, 1024], P('ep', None, 'tp'), may hold values from -1 to 1
- expert_up: bfloat16 [8, 1024, 1024], P('ep', None, 'tp'), may hold values from -1 to 1
- expert_down: bfloat16 [8, 1024, 1024], P('ep', 'tp'), may hold values from -0.1875 to 0.1875
Outputs:
- layer_out: bfloat16 [384, 1024], P('ep', 'tp')
- new_state: float32 [384, 8, 64, 64], P('ep', 'tp')
Inputs may be any that keep to these rules, and one draw needn't show every extreme that they name: `route_experts`: each row names 4 different experts. In each aligned block of 48 rows no expert is named by more than 48 rows, a bound that some block reaches.
All inputs are finite; a program needn't handle non-finite values.
Results may differ from a plain program's by a relative error of at most 0.02.
Values may be sent and summed in bfloat16 or wider, within the bound.
No kernel may reach another device: no remote copies, remote signals or barrier semaphores. Data moves between devices by JAX's collectives and lax.ppermute only.
A program may use at most 128 MiB of HBM per device.

v0:
```python
import jax
import jax.numpy as jnp
from jax import lax
from jax.sharding import PartitionSpec as P

NORM_EPS = 1e-05
GROUP_EPS = 0.00064
UNIT_EPS = 1e-06
CLAMP_LIMIT = 7.0
GLU_ALPHA = 1.702


def row_norm(values):
    return values * lax.rsqrt(jnp.mean(values * values, axis=-1, keepdims=True) + NORM_EPS)


def clamped_unit(gate_pre, up_pre):
    gated = jnp.minimum(gate_pre, CLAMP_LIMIT)
    linear = jnp.clip(up_pre, -CLAMP_LIMIT, CLAMP_LIMIT)
    return gated * jax.nn.sigmoid(GLU_ALPHA * gated) * (linear + 1.0)


def update_heads(head_state, recept, keys, values, decay_rate, rate_gate, head_gain):
    seq_count, head_count, head_size = head_state.shape[:3]

    def by_heads(operand):
        return operand.astype(jnp.float32).reshape(seq_count, head_count, head_size)

    recept_heads = by_heads(recept)
    key_heads = by_heads(keys)
    value_heads = by_heads(values)
    decay_heads = by_heads(decay_rate)
    rate_heads = by_heads(rate_gate)
    unit_key = key_heads * lax.rsqrt(
        jnp.sum(key_heads * key_heads, axis=-1, keepdims=True) + UNIT_EPS
    )
    highest = lax.Precision.HIGHEST
    state_unit = jnp.einsum("shvk,shk->shv", head_state, unit_key, precision=highest)
    new_state = (
        head_state * decay_heads[:, :, None, :]
        - state_unit[..., None] * (unit_key * rate_heads)[:, :, None, :]
        + value_heads[..., None] * (key_heads * rate_heads)[:, :, None, :]
    )
    head_out = jnp.einsum("shvk,shk->shv", new_state, recept_heads, precision=highest)
    centre = jnp.mean(head_out, axis=-1, keepdims=True)
    spread = jnp.mean(jnp.square(head_out - centre), axis=-1, keepdims=True)
    normed_heads = (head_out - centre) * lax.rsqrt(spread + GROUP_EPS)
    mixed = (normed_heads.reshape(seq_count, -1) * head_gain).astype(jnp.bfloat16)
    return (new_state, mixed)


def local(
    tokens,
    head_state,
    recept_weight,
    key_weight,
    value_weight,
    decay_down_factor,
    decay_up_factor,
    decay_base,
    rate_down_factor,
    rate_up_factor,
    rate_base,
    head_gain,
    out_weight,
    route_experts,
    route_weights,
    expert_gate,
    expert_up,
    expert_down,
):
    tokens_float = tokens.astype(jnp.float32)
    normed = row_norm(tokens_float).astype(jnp.bfloat16)
    recept = jnp.dot(normed, recept_weight, preferred_element_type=jnp.float32).astype(jnp.bfloat16)
    keys = jnp.dot(normed, key_weight, preferred_element_type=jnp.float32).astype(jnp.bfloat16)
    values = jnp.dot(normed, value_weight, preferred_element_type=jnp.float32).astype(jnp.bfloat16)
    decay_low = jnp.tanh(
        jnp.dot(normed, decay_down_factor, preferred_element_type=jnp.float32)
    ).astype(jnp.bfloat16)
    rate_low = jnp.dot(normed, rate_down_factor, preferred_element_type=jnp.float32).astype(
        jnp.bfloat16
    )
    decay_pre = decay_base + jnp.dot(decay_low, decay_up_factor, preferred_element_type=jnp.float32)
    decay_rate = jnp.exp(-jnp.exp(-jax.nn.softplus(-decay_pre) - 0.5))
    rate_gate = jax.nn.sigmoid(
        rate_base + jnp.dot(rate_low, rate_up_factor, preferred_element_type=jnp.float32)
    )
    new_state, mixed = update_heads(
        head_state, recept, keys, values, decay_rate, rate_gate, head_gain
    )
    partial_value = jnp.dot(mixed, out_weight, preferred_element_type=jnp.float32).astype(
        jnp.bfloat16
    )
    partial_value = lax.optimization_barrier(partial_value).astype(jnp.float32)
    summed = lax.psum(partial_value.astype(jnp.bfloat16), "tp").astype(jnp.float32)
    residual = (tokens_float + summed).astype(jnp.bfloat16)
    expert_input = row_norm(residual.astype(jnp.float32)).astype(jnp.bfloat16)
    seq_count, top_count = route_experts.shape
    expert_count = lax.axis_size("ep")
    capacity = max(2, (2 * seq_count * top_count + expert_count - 1) // expert_count)
    column_count = expert_input.shape[1] // lax.axis_size("tp")
    column_start = lax.axis_index("tp") * column_count
    flat_routes = route_experts.reshape(-1)
    onehot = (flat_routes[:, None] == jnp.arange(expert_count, dtype=jnp.int32)[None, :]).astype(
        jnp.int32
    )
    earlier = jnp.cumsum(onehot, axis=0) - onehot
    target = flat_routes * capacity + jnp.sum(earlier * onehot, axis=1)
    slot_ids = jnp.arange(expert_count * capacity, dtype=jnp.int32)
    dispatch_map = jnp.any(
        slot_ids[:, None, None] == target.reshape(seq_count, top_count)[None], axis=-1
    )
    dispatch_map = dispatch_map.astype(jnp.bfloat16)
    outgoing = lax.dynamic_slice_in_dim(expert_input, column_start, column_count, 1)
    buffer = jnp.dot(dispatch_map, outgoing, preferred_element_type=jnp.float32).astype(
        jnp.bfloat16
    )
    buffer = buffer.reshape(expert_count, capacity, outgoing.shape[1])
    slot_rows = lax.all_gather(
        lax.all_to_all(buffer, "ep", split_axis=0, concat_axis=0, tiled=True),
        "tp",
        axis=2,
        tiled=True,
    )
    source_count, slot_count, model_width = slot_rows.shape
    flat_rows = slot_rows.reshape(-1, model_width)
    gate_pre = jnp.dot(flat_rows, expert_gate[0], preferred_element_type=jnp.float32)
    up_pre = jnp.dot(flat_rows, expert_up[0], preferred_element_type=jnp.float32)
    activated = clamped_unit(gate_pre, up_pre).astype(jnp.bfloat16)
    part_out = jnp.dot(activated, expert_down[0], preferred_element_type=jnp.float32).astype(
        jnp.bfloat16
    )
    part_out = lax.optimization_barrier(part_out).astype(jnp.float32)
    part_out = part_out.reshape(source_count, slot_count, model_width)
    shares = lax.psum_scatter(part_out.astype(jnp.bfloat16), "tp", scatter_dimension=2, tiled=True)
    returned = lax.all_to_all(shares, "ep", split_axis=0, concat_axis=0, tiled=True)
    picked = returned.reshape(expert_count * capacity, column_count)[target]
    picked = picked.reshape(seq_count, top_count, column_count).astype(jnp.float32)
    mixture = jnp.sum(route_weights[:, :, None] * picked, axis=1)
    own_residual = lax.dynamic_slice_in_dim(residual, column_start, column_count, 1).astype(
        jnp.float32
    )
    layer_out = (own_residual + mixture).astype(jnp.bfloat16)
    return (layer_out, new_state)


def solution(mesh):
    in_specs = (
        P("ep", None),
        P("ep", "tp", None, None),
        P(None, "tp"),
        P(None, "tp"),
        P(None, "tp"),
        P(),
        P(None, "tp"),
        P("tp"),
        P(),
        P(None, "tp"),
        P("tp"),
        P("tp"),
        P("tp", None),
        P("ep", None),
        P("ep", None),
        P("ep", None, "tp"),
        P("ep", None, "tp"),
        P("ep", "tp", None),
    )
    out_specs = (P("ep", "tp"), P("ep", "tp", None, None))
    return jax.shard_map(local, mesh=mesh, in_specs=in_specs, out_specs=out_specs, check_vma=False)
```

profile of v0, /device:TPU:0, one launch (start us, length us, event | category | flops | bytes accessed | tf_op | source)
XLA Modules:
  0.0 132.7 jit_solution(9616172341950078391)
XLA Ops:
  7.2 0.0 all-reduce.3.cloned.1.call-start
  7.2 1.1 fusion.22
  8.3 1.2 fusion.10
  9.5 0.1 reshape.151
  9.6 0.1 multiply_reduce_fusion.3
  9.8 1.3 %fusion.6 = f32[48,128]{1,0:T(8,128)S(1)} fusion(bf16[64,128]{1,0:T(8,128)(2,1)} %param.27, bf16[1024,64]{0,1:T(8,128)(2,1)} %param.26, f32[128]{0:T(128)} %param.28, bf16[48,1024]{1,0:T(8,128)(2,1)} %param.18, f32[48]{0:T(128)S(1)} %add_rsqrt_fusion.3), kind=kOutput, calls=%fused_computation.14 | convolution fusion | flops 7252992 | bytes 271040 | tf_op jit(solution)/shard_map/dot_general | solution.py:86
  11.1 0.1 reshape.142
  11.2 1.4 %fusion.35 = f32[48,128]{1,0:T(8,128)S(1)} fusion(bf16[64,128]{1,0:T(8,128)(2,1)} %param.24, bf16[1024,64]{0,1:T(8,128)(2,1)} %param.23, f32[128]{0:T(128)} %param.25, bf16[48,1024]{1,0:T(8,128)(2,1)} %param.18, f32[48]{0:T(128)S(1)} %add_rsqrt_fusion.3), kind=kOutput, calls=%fused_computation.59 | convolution fusion | flops 7296000 | bytes 271040 | tf_op jit(solution)/shard_map/dot_general | solution.py:83
  12.6 0.1 mul.155
  12.7 1.2 fusion.9
  13.9 0.1 reshape.152
  14.0 1.2 convolution_convert_fusion.3
  15.2 0.1 reshape.168
  15.3 0.1 fusion.54
  15.5 7.0 %fusion.55 = f32[48,2,1,64]{3,2,1,0:T(1,128)S(1)} fusion(f32[48,2,64,1]{2,3,1,0:T(1,128)S(1)} %bitcast.53, f32[48,2,64,64]{3,2,1,0:T(8,128)} %param.19), kind=kOutput, calls=%fused_computation.87 | convolution fusion | flops 4718592 | bytes 1622016 | tf_op jit(solution)/shard_map/shvk,shk->shv/dot_general | solution.py:38
  22.5 2.1 %multiply_add_fusion = f32[48,2,64,64]{3,2,1,0:T(8,128)S(1)} fusion(f32[48,2,64,64]{3,2,1,0:T(8,128)S(1)} %copy-done.1, f32[48,2,64]{2,1,0:T(2,128)S(1)} %get-tuple-element.6, f32[48,2,64]{2,1,0:T(2,128)S(1)} %reshape.152, f32[48,2,64]{2,1,0:T(2,128)S(1)} %get-tuple-element.4, f32[48,2,64]{2,1,0:T(2,128)S(1)} %bitcast.52, f32[48,2,64]{2,1,0:T(2,128)S(1)} %mul.155), kind=kLoop, calls=%fused_computation.1 | loop fusion | flops 1966080 | bytes 3268608 | tf_op jit(solution)/shard_map/add | solution.py:40
  24.6 1.7 %copy-done.2 = f32[48,2,64,64]{3,2,1,0:T(8,128)} copy-done((f32[48,2,64,64]{3,2,1,0:T(8,128)}, f32[48,2,64,64]{3,2,1,0:T(8,128)S(1)}, u32[]{:S(2)}) %copy-start.2) | copy-done | bytes 1572888
  26.2 2.5 %fusion.56 = f32[48,2,1,64]{3,2,1,0:T(1,128)S(1)} fusion(f32[48,2,64,64]{3,2,1,0:T(8,128)S(1)} %multiply_add_fusion, bf16[48,2,64,1]{2,3,1,0:T(2,128)(2,1)S(1)} %reshape.168), kind=kOutput, calls=%fused_computation.88 | convolution fusion | flops 4718592 | bytes 1609728 | tf_op jit(solution)/shard_map/shvk,shk->shv/dot_general | solution.py:44
  28.8 0.1 reduce_sum.69
  28.9 0.2 multiply_reduce_fusion.2
  29.2 0.2 subtract_multiply_fusion
  29.3 0.1 reshape.144
  29.4 0.8 convolution_convert_fusion.2
  30.2 0.0 all-reduce.3.cloned.1.call-update
  30.3 0.0 reduce-scatter.2.cloned.1.call-start
  30.3 0.1 copy.34
  30.4 0.1 eq.36
  30.6 0.6 reduce-window.6
  31.1 0.2 slice_reduce_fusion
  31.4 0.1 add_bitcast_fusion
  31.5 0.1 reduce_sum.72
  31.6 0.1 copy.36
  31.7 0.1 fusion.21
  31.8 33.0 %all-reduce.3.cloned.1.call-done = bf16[48,1024]{1,0:T(8,128)(2,1)} async-done(((bf16[48,1024]{1,0:T(8,128)(2,1)}), bf16[48,1024]{1,0:T(8,128)(2,1)}) %all-reduce.3.cloned.1.call-update) | async-done | bytes 98320 | tf_op jit(solution)/shard_map/psum | solution.py:95
  64.8 1.0 multiply_reduce_fusion.1
  65.9 0.3 convolution_convert_fusion.1
  66.2 13.1 %all_to_all.10 = bf16[8,48,256]{2,1,0:T(8,128)(2,1)S(1)} all-to-all(bf16[8,48,256]{2,1,0:T(8,128)(2,1)S(1)} %bitcast.48), channel_id=1, replica_groups=mesh['ep'=8,'tp'=4] {'ep'}, dimensions={0} | all-to-all | bytes 393216 | tf_op jit(solution)/shard_map/all_to_all | solution.py:120
  79.3 7.6 %all_gather.3 = bf16[8,48,1024]{2,1,0:T(8,128)(2,1)S(1)} all-gather(bf16[8,48,256]{2,1,0:T(8,128)(2,1)S(1)} %all_to_all.10), channel_id=1, replica_groups=mesh['ep'=8,'tp'=4] {'tp'}, dimensions={2}, use_global_device_ids=true | all-gather | bytes 983040 | tf_op jit(solution)/shard_map/all_gather | solution.py:119
  86.9 0.4 convolution_minimum_fusion
  87.3 1.9 %convolution_convert_fusion = bf16[384,1024]{1,0:T(8,128)(2,1)} fusion(bf16[384,1024]{1,0:T(8,128)(2,1)S(1)} %bitcast.46, bf16[1,256,1024]{2,1,0:T(8,128)(2,1)S(1)} %copy-done, bf16[1,1024,256]{2,1,0:T(8,128)(2,1)S(1)} %copy-done.9, f32[384,256]{1,0:T(8,128)S(1)} %convolution_minimum_fusion), kind=kOutput, calls=%fused_computation.2 | convolution fusion | flops 403931136 | bytes 3014656 | tf_op jit(solution)/shard_map/dot_general | solution.py:130
  89.2 21.5 %reduce-scatter.2.cloned.1.call-done = bf16[8,48,256]{2,1,0:T(8,128)(2,1)} async-done(((bf16[8,48,1024]{2,1,0:T(8,128)(2,1)}), bf16[8,48,256]{2,1,0:T(8,128)(2,1)}) %reduce-scatter.2.cloned.1.call-update) | async-done | bytes 196624 | tf_op jit(solution)/shard_map/reduce_scatter | solution.py:135
  110.6 5.5 %all-to-all-start.1 = ((bf16[8,48,256]{2,1,0:T(8,128)(2,1)}), bf16[8,48,256]{2,1,0:T(8,128)(2,1)S(1)}, u32[]{:S(2)}, u32[]{:S(2)}) async-start(bf16[8,48,256]{2,1,0:T(8,128)(2,1)} %reduce-scatter.2.cloned.1.call-done), calls=%async_computation.2 | async-start | bytes 393216 | tf_op jit(solution)/shard_map/all_to_all | solution.py:136
  116.2 0.1 mul.187
  116.3 0.1 copy.33
  116.4 7.6 %all-to-all-done.1 = bf16[8,48,256]{2,1,0:T(8,128)(2,1)S(1)} async-done(((bf16[8,48,256]{2,1,0:T(8,128)(2,1)}), bf16[8,48,256]{2,1,0:T(8,128)(2,1)S(1)}, u32[]{:S(2)}, u32[]{:S(2)}) %all-to-all-start.1) | async-done | bytes 196640 | tf_op jit(solution)/shard_map/all_to_all | solution.py:136
  123.9 1.0 gather_fusion
  125.0 0.2 multiply_reduce_fusion
  125.2 0.6 add_convert_fusion
  (35 shorter events, 0.3 us)
Async XLA Ops:
  7.2 80.1 %copy-start = (bf16[1,256,1024]{2,1,0:T(8,128)(2,1)S(1)}, bf16[1,256,1024]{2,1,0:T(8,128)(2,1)}, u32[]{:S(2)}) copy-start(bf16[1,256,1024]{2,1,0:T(8,128)(2,1)} %param.35) | copy-start | bytes 1572868
  7.2 57.6 %all-reduce.3.cloned.1.call-start = ((), (), s32[]{:S(2)}) async-start(), calls=%async_computation.3 | async-start | bytes 196608 | tf_op jit(solution)/shard_map/psum | solution.py:95
  15.3 7.2 %copy-start.1 = (f32[48,2,64,64]{3,2,1,0:T(8,128)S(1)}, f32[48,2,64,64]{3,2,1,0:T(8,128)}, u32[]{:S(2)}) copy-start(f32[48,2,64,64]{3,2,1,0:T(8,128)} %param.19) | copy-start | bytes 4718596
  24.6 1.7 %copy-start.2 = (f32[48,2,64,64]{3,2,1,0:T(8,128)}, f32[48,2,64,64]{3,2,1,0:T(8,128)S(1)}, u32[]{:S(2)}) copy-start(f32[48,2,64,64]{3,2,1,0:T(8,128)S(1)} %multiply_add_fusion) | copy-start | bytes 4718596
  26.2 3.2 %copy-start.5 = (bf16[128,1024]{1,0:T(8,128)(2,1)S(1)}, bf16[128,1024]{1,0:T(8,128)(2,1)}, u32[]{:S(2)}) copy-start(bf16[128,1024]{1,0:T(8,128)(2,1)} %param.30) | copy-start | bytes 786436
  26.2 3.2 %copy-start.8 = (f32[128]{0:T(128)S(1)}, f32[128]{0:T(128)}, u32[]{:S(2)}) copy-start(f32[128]{0:T(128)} %param.29) | copy-start | bytes 1540
  26.2 4.1 %copy-start.6 = (s32[48,4]{0,1:T(4,128)S(1)}, s32[48,4]{0,1:T(4,128)}, u32[]{:S(2)}) copy-start(s32[48,4]{0,1:T(4,128)} %param.31) | copy-start | bytes 2308
  26.2 38.6 %copy-start.3 = (bf16[48,1024]{1,0:T(8,128)(2,1)S(1)}, bf16[48,1024]{1,0:T(8,128)(2,1)}, u32[]{:S(2)}) copy-start(bf16[48,1024]{1,0:T(8,128)(2,1)} %param.18) | copy-start | bytes 294916
  26.2 60.6 %copy-start.4 = (bf16[1,1024,256]{2,1,0:T(8,128)(2,1)S(1)}, bf16[1,1024,256]{2,1,0:T(8,128)(2,1)}, u32[]{:S(2)}) copy-start(bf16[1,1024,256]{2,1,0:T(8,128)(2,1)} %param.33) | copy-start | bytes 1572868
  28.8 58.5 %copy-start.9 = (bf16[1,1024,256]{2,1,0:T(8,128)(2,1)S(1)}, bf16[1,1024,256]{2,1,0:T(8,128)(2,1)}, u32[]{:S(2)}) copy-start(bf16[1,1024,256]{2,1,0:T(8,128)(2,1)} %param.34) | copy-start | bytes 1572868
  30.3 80.4 %reduce-scatter.2.cloned.1.call-start = ((), (), s32[]{:S(2)}) async-start(), calls=%async_computation.4 | async-start | bytes 983040 | tf_op jit(solution)/shard_map/reduce_scatter | solution.py:135
  87.3 29.0 %copy-start.7 = (f32[48,4]{0,1:T(4,128)S(1)}, f32[48,4]{0,1:T(4,128)}, u32[]{:S(2)}) copy-start(f32[48,4]{0,1:T(4,128)} %param.32) | copy-start | bytes 2308
  110.6 13.3 %all-to-all-start.1 = ((bf16[8,48,256]{2,1,0:T(8,128)(2,1)}), bf16[8,48,256]{2,1,0:T(8,128)(2,1)S(1)}, u32[]{:S(2)}, u32[]{:S(2)}) async-start(bf16[8,48,256]{2,1,0:T(8,128)(2,1)} %reduce-scatter.2.cloned.1.call-done), calls=%async_computation.2 | async-start | bytes 393216 | tf_op jit(solution)/shard_map/all_to_all | solution.py:136
Sparse Core Ops, SparseCore 0:
  30.4 34.3 all-reduce.2
  89.3 21.2 reduce-scatter.1
where the time goes:
time: 133 us
  waiting for transfers between devices  62 us (47%)
  blocking collectives  20.7 us (16%)
  matrix products  19.3 us (15%)
  between operations  14.4 us (11%)
  other arithmetic  6.64 us (5%)
  starting transfers between devices  5.59 us (4%)
  local copies, waits for them, and re-layouts  4.08 us (3%)
    psum x1, waiting for transfers between devices, local(): lax.psum(partial_value.astype(jnp.bfloat16), 'tp').astype(jnp.float32)  33 us
    reduce_scatter x1, waiting for transfers between devices, local(): lax.psum_scatter(part_out.astype(jnp.bfloat16), 'tp', scatter_dimension=2...  21.5 us
    all_to_all x1, blocking collectives, local(): lax.all_to_all(buffer, 'ep', split_axis=0, concat_axis=0, tiled=True)  13.1 us
    all_gather x1, blocking collectives, local(): lax.all_gather(lax.all_to_all(buffer, 'ep', split_axis=0, concat_axis=0,...  7.58 us
    all_to_all x1, waiting for transfers between devices, local(): lax.all_to_all(shares, 'ep', split_axis=0, concat_axis=0, tiled=True)  7.57 us
    dot_general x1, matrix products, update_heads(): jnp.einsum('shvk,shk->shv', head_state, unit_key, precision=highest)  7.01 us
    all_to_all x1, starting transfers between devices, local(): lax.all_to_all(shares, 'ep', split_axis=0, concat_axis=0, tiled=True)  5.51 us
  transfers between devices with their start and end apart: 3, of which 3 were waited for; matrix products, arithmetic and copies ran while one was open for 1% of the time, Pallas kernels for 0%

commit v1 on v0

--- a/solution.py
+++ b/solution.py
@@ -116,11 +116,9 @@
         jnp.bfloat16
     )
     buffer = buffer.reshape(expert_count, capacity, outgoing.shape[1])
-    slot_rows = lax.all_gather(
-        lax.all_to_all(buffer, "ep", split_axis=0, concat_axis=0, tiled=True),
-        "tp",
+    slot_rows = jnp.concatenate(
+        lax.all_gather(lax.all_to_all(buffer, "ep", split_axis=0, concat_axis=0, tiled=True), "tp"),
         axis=2,
-        tiled=True,
     )
     source_count, slot_count, model_width = slot_rows.shape
     flat_rows = slot_rows.reshape(-1, model_width)

time: 133 us -> 134 us (level)
  no operation moved by 1% of the time
where the time goes in v1:
time: 134 us
  waiting for transfers between devices  62 us (46%)
  blocking collectives  20.8 us (16%)
  matrix products  19.3 us (14%)
  between operations  14.4 us (11%)
  other arithmetic  6.64 us (5%)
  starting transfers between devices  5.59 us (4%)
  local copies, waits for them, and re-layouts  4.84 us (4%)
    psum x1, waiting for transfers between devices, local(): lax.psum(partial_value.astype(jnp.bfloat16), 'tp').astype(jnp.float32)  33 us
    reduce_scatter x1, waiting for transfers between devices, local(): lax.psum_scatter(part_out.astype(jnp.bfloat16), 'tp', scatter_dimension=2...  21.5 us
    all_to_all x1, blocking collectives, local(): lax.all_to_all(buffer, 'ep', split_axis=0, concat_axis=0, tiled=True)  13.2 us
    all_gather x1, blocking collectives, local(): lax.all_gather(lax.all_to_all(buffer, 'ep', split_axis=0, concat_axis=0,...  7.58 us
    all_to_all x1, waiting for transfers between devices, local(): lax.all_to_all(shares, 'ep', split_axis=0, concat_axis=0, tiled=True)  7.57 us
    dot_general x1, matrix products, update_heads(): jnp.einsum('shvk,shk->shv', head_state, unit_key, precision=highest)  7.01 us
    all_to_all x1, starting transfers between devices, local(): lax.all_to_all(shares, 'ep', split_axis=0, concat_axis=0, tiled=True)  5.51 us
  transfers between devices with their start and end apart: 3, of which 3 were waited for; matrix products, arithmetic and copies ran while one was open for 1% of the time, Pallas kernels for 0%

profile of v1, /device:TPU:0, one launch (start us, length us, event | category | flops | bytes accessed | tf_op | source)
XLA Modules:
  0.0 133.6 jit_solution(3989017997268242690)
XLA Ops:
  7.2 1.1 fusion.22
  8.3 1.2 fusion.10
  9.5 0.1 reshape.151
  9.6 0.1 multiply_reduce_fusion.3
  9.8 1.3 fusion.6
  11.1 0.1 reshape.142
  11.2 1.4 %fusion.35 = f32[48,128]{1,0:T(8,128)S(1)} fusion(bf16[64,128]{1,0:T(8,128)(2,1)} %param.24, bf16[1024,64]{0,1:T(8,128)(2,1)} %param.23, f32[128]{0:T(128)} %param.25, bf16[48,1024]{1,0:T(8,128)(2,1)} %param.18, f32[48]{0:T(128)S(1)} %add_rsqrt_fusion.3), kind=kOutput, calls=%fused_computation.59 | convolution fusion | flops 7296000 | bytes 271040 | tf_op jit(solution)/shard_map/dot_general | solution.py:83
  12.6 0.1 mul.155
  12.7 1.2 fusion.9
  13.9 0.1 reshape.152
  14.0 1.2 convolution_convert_fusion.3
  15.2 0.1 reshape.169
  15.3 0.1 fusion.54
  15.5 7.0 %fusion.55 = f32[48,2,1,64]{3,2,1,0:T(1,128)S(1)} fusion(f32[48,2,64,1]{2,3,1,0:T(1,128)S(1)} %bitcast.60, f32[48,2,64,64]{3,2,1,0:T(8,128)} %param.19), kind=kOutput, calls=%fused_computation.87 | convolution fusion | flops 4718592 | bytes 1622016 | tf_op jit(solution)/shard_map/shvk,shk->shv/dot_general | solution.py:38
  22.5 2.1 %multiply_add_fusion = f32[48,2,64,64]{3,2,1,0:T(8,128)S(1)} fusion(f32[48,2,64,64]{3,2,1,0:T(8,128)S(1)} %copy-done.1, f32[48,2,64]{2,1,0:T(2,128)S(1)} %get-tuple-element.6, f32[48,2,64]{2,1,0:T(2,128)S(1)} %reshape.152, f32[48,2,64]{2,1,0:T(2,128)S(1)} %get-tuple-element.4, f32[48,2,64]{2,1,0:T(2,128)S(1)} %bitcast.59, f32[48,2,64]{2,1,0:T(2,128)S(1)} %mul.155), kind=kLoop, calls=%fused_computation.1 | loop fusion | flops 1966080 | bytes 3268608 | tf_op jit(solution)/shard_map/add | solution.py:40
  24.6 1.7 %copy-done.2 = f32[48,2,64,64]{3,2,1,0:T(8,128)} copy-done((f32[48,2,64,64]{3,2,1,0:T(8,128)}, f32[48,2,64,64]{3,2,1,0:T(8,128)S(1)}, u32[]{:S(2)}) %copy-start.2) | copy-done | bytes 1572888
  26.2 2.5 %fusion.56 = f32[48,2,1,64]{3,2,1,0:T(1,128)S(1)} fusion(f32[48,2,64,64]{3,2,1,0:T(8,128)S(1)} %multiply_add_fusion, bf16[48,2,64,1]{2,3,1,0:T(2,128)(2,1)S(1)} %reshape.169), kind=kOutput, calls=%fused_computation.88 | convolution fusion | flops 4718592 | bytes 1609728 | tf_op jit(solution)/shard_map/shvk,shk->shv/dot_general | solution.py:44
  28.8 0.1 reduce_sum.69
  28.9 0.2 multiply_reduce_fusion.2
  29.2 0.2 subtract_multiply_fusion
  29.3 0.1 reshape.144
  29.4 0.8 convolution_convert_fusion.2
  30.3 0.0 reduce-scatter.2.cloned.1.call-start
  30.3 0.1 copy.43
  30.4 0.1 eq.36
  30.6 0.6 reduce-window.6
  31.1 0.2 slice_reduce_fusion
  31.4 0.1 add_bitcast_fusion
  31.5 0.1 reduce_sum.72
  31.6 0.1 copy.45
  31.7 0.1 fusion.21
  31.8 33.0 %all-reduce.3.cloned.1.call-done = bf16[48,1024]{1,0:T(8,128)(2,1)} async-done(((bf16[48,1024]{1,0:T(8,128)(2,1)}), bf16[48,1024]{1,0:T(8,128)(2,1)}) %all-reduce.3.cloned.1.call-update) | async-done | bytes 98320 | tf_op jit(solution)/shard_map/psum | solution.py:95
  64.8 1.0 multiply_reduce_fusion.1
  65.9 0.3 convolution_convert_fusion.1
  66.2 13.2 %all_to_all.10 = bf16[8,48,256]{2,1,0:T(8,128)(2,1)S(1)} all-to-all(bf16[8,48,256]{2,1,0:T(8,128)(2,1)S(1)} %bitcast.55), channel_id=1, replica_groups=mesh['ep'=8,'tp'=4] {'ep'}, dimensions={0} | all-to-all | bytes 393216 | tf_op jit(solution)/shard_map/all_to_all | solution.py:120
  79.4 7.6 %all-gather = bf16[32,48,256]{2,1,0:T(8,128)(2,1)S(1)} all-gather(bf16[8,48,256]{2,1,0:T(8,128)(2,1)S(1)} %all_to_all.10), channel_id=2, replica_groups=mesh['ep'=8,'tp'=4] {'tp'}, dimensions={0}, use_global_device_ids=true | all-gather | bytes 983040 | tf_op jit(solution)/shard_map/all_gather | solution.py:120
  87.0 0.6 copy.46
  87.6 0.2 copy.53
  87.8 0.4 convolution_minimum_fusion
  88.2 1.9 %convolution_convert_fusion = bf16[384,1024]{1,0:T(8,128)(2,1)} fusion(bf16[384,1024]{1,0:T(8,128)(2,1)S(1)} %bitcast.52, bf16[1,256,1024]{2,1,0:T(8,128)(2,1)S(1)} %copy-done, bf16[1,1024,256]{2,1,0:T(8,128)(2,1)S(1)} %copy-done.9, f32[384,256]{1,0:T(8,128)S(1)} %convolution_minimum_fusion), kind=kOutput, calls=%fused_computation.2 | convolution fusion | flops 403931136 | bytes 3014656 | tf_op jit(solution)/shard_map/dot_general | solution.py:128
  90.1 21.5 %reduce-scatter.2.cloned.1.call-done = bf16[8,48,256]{2,1,0:T(8,128)(2,1)} async-done(((bf16[8,48,1024]{2,1,0:T(8,128)(2,1)}), bf16[8,48,256]{2,1,0:T(8,128)(2,1)}) %reduce-scatter.2.cloned.1.call-update) | async-done | bytes 196624 | tf_op jit(solution)/shard_map/reduce_scatter | solution.py:133
  111.6 5.5 %all-to-all-start.1 = ((bf16[8,48,256]{2,1,0:T(8,128)(2,1)}), bf16[8,48,256]{2,1,0:T(8,128)(2,1)S(1)}, u32[]{:S(2)}, u32[]{:S(2)}) async-start(bf16[8,48,256]{2,1,0:T(8,128)(2,1)} %reduce-scatter.2.cloned.1.call-done), calls=%async_computation.2 | async-start | bytes 393216 | tf_op jit(solution)/shard_map/all_to_all | solution.py:134
  117.1 0.1 mul.187
  117.2 0.1 copy.42
  117.3 7.6 %all-to-all-done.1 = bf16[8,48,256]{2,1,0:T(8,128)(2,1)S(1)} async-done(((bf16[8,48,256]{2,1,0:T(8,128)(2,1)}), bf16[8,48,256]{2,1,0:T(8,128)(2,1)S(1)}, u32[]{:S(2)}, u32[]{:S(2)}) %all-to-all-start.1) | async-done | bytes 196640 | tf_op jit(solution)/shard_map/all_to_all | solution.py:134
  124.9 1.0 gather_fusion
  125.9 0.2 multiply_reduce_fusion
  126.1 0.6 add_convert_fusion
  (37 shorter events, 0.3 us)
Async XLA Ops:
  7.2 81.0 %copy-start = (bf16[1,256,1024]{2,1,0:T(8,128)(2,1)S(1)}, bf16[1,256,1024]{2,1,0:T(8,128)(2,1)}, u32[]{:S(2)}) copy-start(bf16[1,256,1024]{2,1,0:T(8,128)(2,1)} %param.35) | copy-start | bytes 1572868
  7.2 57.6 %all-reduce.3.cloned.1.call-start = ((), (), s32[]{:S(2)}) async-start(), calls=%async_computation.3 | async-start | bytes 196608 | tf_op jit(solution)/shard_map/psum | solution.py:95
  15.3 7.2 %copy-start.1 = (f32[48,2,64,64]{3,2,1,0:T(8,128)S(1)}, f32[48,2,64,64]{3,2,1,0:T(8,128)}, u32[]{:S(2)}) copy-start(f32[48,2,64,64]{3,2,1,0:T(8,128)} %param.19) | copy-start | bytes 4718596
  24.6 1.7 %copy-start.2 = (f32[48,2,64,64]{3,2,1,0:T(8,128)}, f32[48,2,64,64]{3,2,1,0:T(8,128)S(1)}, u32[]{:S(2)}) copy-start(f32[48,2,64,64]{3,2,1,0:T(8,128)S(1)} %multiply_add_fusion) | copy-start | bytes 4718596
  26.2 3.2 %copy-start.5 = (bf16[128,1024]{1,0:T(8,128)(2,1)S(1)}, bf16[128,1024]{1,0:T(8,128)(2,1)}, u32[]{:S(2)}) copy-start(bf16[128,1024]{1,0:T(8,128)(2,1)} %param.30) | copy-start | bytes 786436
  26.2 3.2 %copy-start.8 = (f32[128]{0:T(128)S(1)}, f32[128]{0:T(128)}, u32[]{:S(2)}) copy-start(f32[128]{0:T(128)} %param.29) | copy-start | bytes 1540
  26.2 4.1 %copy-start.6 = (s32[48,4]{0,1:T(4,128)S(1)}, s32[48,4]{0,1:T(4,128)}, u32[]{:S(2)}) copy-start(s32[48,4]{0,1:T(4,128)} %param.31) | copy-start | bytes 2308
  26.2 38.6 %copy-start.3 = (bf16[48,1024]{1,0:T(8,128)(2,1)S(1)}, bf16[48,1024]{1,0:T(8,128)(2,1)}, u32[]{:S(2)}) copy-start(bf16[48,1024]{1,0:T(8,128)(2,1)} %param.18) | copy-start | bytes 294916
  29.3 58.5 %copy-start.4 = (bf16[1,1024,256]{2,1,0:T(8,128)(2,1)S(1)}, bf16[1,1024,256]{2,1,0:T(8,128)(2,1)}, u32[]{:S(2)}) copy-start(bf16[1,1024,256]{2,1,0:T(8,128)(2,1)} %param.33) | copy-start | bytes 1572868
  30.3 81.3 %reduce-scatter.2.cloned.1.call-start = ((), (), s32[]{:S(2)}) async-start(), calls=%async_computation.4 | async-start | bytes 983040 | tf_op jit(solution)/shard_map/reduce_scatter | solution.py:133
  66.2 22.0 %copy-start.9 = (bf16[1,1024,256]{2,1,0:T(8,128)(2,1)S(1)}, bf16[1,1024,256]{2,1,0:T(8,128)(2,1)}, u32[]{:S(2)}) copy-start(bf16[1,1024,256]{2,1,0:T(8,128)(2,1)} %param.34) | copy-start | bytes 1572868
  88.2 29.0 %copy-start.7 = (f32[48,4]{0,1:T(4,128)S(1)}, f32[48,4]{0,1:T(4,128)}, u32[]{:S(2)}) copy-start(f32[48,4]{0,1:T(4,128)} %param.32) | copy-start | bytes 2308
  111.6 13.3 %all-to-all-start.1 = ((bf16[8,48,256]{2,1,0:T(8,128)(2,1)}), bf16[8,48,256]{2,1,0:T(8,128)(2,1)S(1)}, u32[]{:S(2)}, u32[]{:S(2)}) async-start(bf16[8,48,256]{2,1,0:T(8,128)(2,1)} %reduce-scatter.2.cloned.1.call-done), calls=%async_computation.2 | async-start | bytes 393216 | tf_op jit(solution)/shard_map/all_to_all | solution.py:134
Sparse Core Ops, SparseCore 0:
  30.4 34.3 all-reduce.2
  90.2 21.2 reduce-scatter.1
